TPU v7x, 32 devices: a whole 2x2x4 slice. The times are simulated.
32 devices in a mesh: sp: 4 (over z), fs: 4 (over y, x), tp: 2 (over core).
Axes of the slice: x: 2, y: 2, z: 4, core: 2. Of those that a mesh axis runs over, the one named last changes fastest.
Arguments:
- tokens: bfloat16 [8, 1536, 2048], P('fs', ('sp', 'tp')), may hold values from -6 to 6
- norm_gain: float32 [2048], replicated, may hold values from 0.1 to 1.9
- chain_entry: bfloat16 [2048, 2048], P(('sp', 'fs'), 'tp'), may hold values from -0.125 to 0.125
- pool_entry: bfloat16 [2048, 2048], P(('sp', 'fs'), 'tp'), may hold values from -0.125 to 0.125
- conv_taps: bfloat16 [4, 2048], P(None, 'tp'), may hold values from -3 to 3
- recur_gate: bfloat16 [8, 256, 256], P('tp'), may hold values from -0.375 to 0.375
- input_gate: bfloat16 [8, 256, 256], P('tp'), may hold values from -0.375 to 0.375
- decay_log: float32 [2048], P('tp'), may hold values from -9 to 5
- decay_shift: float32 [8, 1536, 2048], P('fs', 'sp', 'tp'), may hold values from -1 to 0
- start_state: float32 [8, 2048], P('fs', 'tp'), may hold values from -6 to 6
- pool_mix: bfloat16 [8, 256, 256], P('tp'), may hold values from -0.375 to 0.375
- pool_scale: float32 [2048], P('tp'), may hold values from 0.1 to 1.9
- chain_exit: bfloat16 [2048, 2048], P('tp', ('sp', 'fs')), may hold values from -0.09375 to 0.09375
- pool_exit: bfloat16 [2048, 2048], P('tp', ('sp', 'fs')), may hold values from -0.09375 to 0.09375
Outputs:
- mixed_rows: bfloat16 [8, 1536, 2048], P('fs', ('sp', 'tp'))
All inputs are finite; a program needn't handle non-finite values.
Results may differ from a plain program's by a relative error of at most 0.01.
Values may be sent and summed in bfloat16 or wider, within the bound.
A program may use at most 128 MiB of HBM per device.

v0:
```python
import jax
import jax.numpy as jnp
from jax import lax
from jax.sharding import PartitionSpec as P

POOL_SPAN = 16


NORM_EPSILON = 1e-06
RECUR_SCALE = 8.0


def passed_along(shard, axis, by):
    devices = lax.axis_size(axis)
    pairs = [(i, i + by) for i in range(devices) if 0 <= i + by < devices]
    return lax.ppermute(shard, axis, pairs)


def carried_in(part, axis, combine, identity):
    place = lax.axis_index(axis)
    gathered = jax.tree.map(lambda a: lax.all_gather(a, axis), part)
    state = jax.tree.map(lambda a, e: jnp.zeros_like(a) + jnp.asarray(e, a.dtype), part, identity)

    def one(lap, state):
        return combine(
            state, jax.tree.map(lambda a: lax.dynamic_index_in_dim(a, lap, 0, False), gathered)
        )

    return lax.fori_loop(0, place, one, state)


def block_map(values, weight):
    groups, block_width, _ = weight.shape
    lead = values.shape[:-1]
    mapped = jnp.einsum(
        "...gi,gij->...gj",
        values.reshape(lead + (groups, block_width)),
        weight,
        preferred_element_type=jnp.float32,
    )
    return mapped.reshape(lead + (groups * block_width,))


def combine(earlier, latter):
    return (earlier[0] * latter[0], latter[0] * earlier[1] + latter[1])


def trailing(padded, row_total, window_id):
    sum_two = padded[:, 1:] + padded[:, :-1]
    sum_four = sum_two[:, 2:] + sum_two[:, :-2]
    sum_eight = sum_four[:, 4:] + sum_four[:, :-4]
    sixteen = sum_eight[:, 8:] + sum_eight[:, :-8]
    return jnp.where(
        window_id == 0,
        sum_two[:, -row_total:],
        jnp.where(
            window_id == 1,
            sum_four[:, -row_total:],
            jnp.where(window_id == 2, sum_eight[:, -row_total:], sixteen),
        ),
    )


def per_device(
    tokens,
    norm_gain,
    chain_entry,
    pool_entry,
    conv_taps,
    recur_gate,
    input_gate,
    decay_log,
    decay_shift,
    start_state,
    pool_mix,
    pool_scale,
    chain_exit,
    pool_exit,
):
    widened = lax.all_gather(tokens, "tp", axis=1, tiled=True).astype(jnp.float32)
    scaled = (
        widened
        * lax.rsqrt(jnp.mean(widened * widened, axis=-1, keepdims=True) + NORM_EPSILON)
        * norm_gain
    )
    normed = scaled.astype(jnp.bfloat16)
    seq_count = normed.shape[0]
    row_count = normed.shape[1]
    chain_width = chain_entry.shape[1]
    pool_width = pool_entry.shape[1]
    sum_chain = jnp.dot(
        normed,
        lax.all_gather(chain_entry, ("sp", "fs"), axis=0, tiled=True),
        preferred_element_type=jnp.float32,
    )
    sum_pool = jnp.dot(
        normed,
        lax.all_gather(pool_entry, ("sp", "fs"), axis=0, tiled=True),
        preferred_element_type=jnp.float32,
    )
    chain_input = sum_chain.astype(jnp.bfloat16)
    pool_input = sum_pool.astype(jnp.bfloat16)
    tap_count = conv_taps.shape[0]
    prior_chain, prior_pool = passed_along(
        (
            chain_input[:, row_count - (tap_count - 1) :],
            pool_input[:, row_count - (POOL_SPAN - 1) :],
        ),
        "sp",
        1,
    )
    padded = jnp.concatenate([prior_chain, chain_input], axis=1).astype(jnp.float32)
    conv_out = padded[:, 0:row_count] * conv_taps[0].astype(jnp.float32)
    for offset in range(1, tap_count):
        conv_out = conv_out + padded[:, offset : offset + row_count] * conv_taps[offset].astype(
            jnp.float32
        )
    conv_out = conv_out.astype(jnp.bfloat16)
    gate_recur = jax.nn.sigmoid(block_map(conv_out, recur_gate))
    gate_input = jax.nn.sigmoid(block_map(conv_out, input_gate))
    length = row_count * lax.axis_size("sp")
    log_decay = -RECUR_SCALE * gate_recur * (jnp.exp(decay_log) / length) + decay_shift
    decay_factor = jnp.exp(log_decay)
    drive_term = jnp.sqrt(-jnp.expm1(2.0 * log_decay)) * gate_input * conv_out.astype(jnp.float32)
    cum_decay, cum_drive = lax.associative_scan(combine, (decay_factor, drive_term), axis=1)
    identity = (
        jnp.ones((seq_count, chain_width), jnp.float32),
        jnp.zeros((seq_count, chain_width), jnp.float32),
    )
    before_decay, before_drive = carried_in(
        (cum_decay[:, -1], cum_drive[:, -1]), "sp", combine, identity
    )
    entering = before_decay * start_state + before_drive
    recurrent = (cum_decay * entering[:, None, :] + cum_drive).astype(jnp.bfloat16)
    block_width = pool_mix.shape[1]
    first_group = lax.axis_index("tp") * (pool_width // block_width)
    group_index = first_group + jnp.arange(pool_width, dtype=jnp.int32) // block_width
    window_id = (group_index % 4)[None, :]
    window = jnp.power(2.0, (window_id + 1).astype(jnp.float32))
    position = (lax.axis_index("sp") * row_count + jnp.arange(row_count, dtype=jnp.int32)).astype(
        jnp.float32
    )[:, None]
    counts = jnp.minimum(position + 1.0, window)
    pool_pad = jnp.concatenate([prior_pool, pool_input], axis=1).astype(jnp.float32)
    trail_sum = trailing(pool_pad, row_count, window_id)
    pool_diff = (trail_sum / counts - pool_input.astype(jnp.float32)).astype(jnp.bfloat16)
    pooled = (block_map(pool_diff, pool_mix) * pool_scale).astype(jnp.bfloat16)
    recurrent_rows = jnp.transpose(recurrent, (1, 0, 2))
    pooled_rows = jnp.transpose(pooled, (1, 0, 2))
    full_chain, full_pool = (
        lax.all_gather(chain_exit, ("sp", "fs"), axis=1, tiled=True),
        lax.all_gather(pool_exit, ("sp", "fs"), axis=1, tiled=True),
    )
    mixed_rows = lax.psum_scatter(
        jnp.dot(recurrent_rows, full_chain, preferred_element_type=jnp.float32)
        + jnp.dot(pooled_rows, full_pool, preferred_element_type=jnp.float32),
        "tp",
        scatter_dimension=0,
        tiled=True,
    )
    return jnp.transpose(mixed_rows, (1, 0, 2)).astype(jnp.bfloat16)


def solution(mesh):
    in_specs = (
        P("fs", ("sp", "tp"), None),
        P(),
        P(("sp", "fs"), "tp"),
        P(("sp", "fs"), "tp"),
        P(None, "tp"),
        P("tp", None, None),
        P("tp", None, None),
        P("tp"),
        P("fs", "sp", "tp"),
        P("fs", "tp"),
        P("tp", None, None),
        P("tp"),
        P("tp", ("sp", "fs")),
        P("tp", ("sp", "fs")),
    )
    out_specs = P("fs", ("sp", "tp"), None)
    return jax.shard_map(
        per_device, mesh=mesh, in_specs=in_specs, out_specs=out_specs, check_vma=False
    )
```

profile of v0, /device:TPU:11, one launch (start us, length us, event | category | flops | bytes accessed | tf_op | source)
XLA Modules:
  0.0 510.5 jit_solution(15011006323595819352)
XLA Ops:
  14.1 8.7 %all-gather.8.cloned.1.call-done = bf16[2,384,2048]{2,1,0:T(8,128)(2,1)} async-done(((bf16[2,192,2048]{2,1,0:T(8,128)(2,1)}), bf16[2,384,2048]{2,1,0:T(8,128)(2,1)}) %all-gather.8.cloned.1.call-update) | async-done | bytes 3145744 | tf_op jit(solution)/shard_map/all_gather | solution.py:80
  22.9 2.6 fusion
  25.5 75.0 %all-gather.10.cloned.1.call-done = bf16[2048,1024]{1,0:T(8,128)(2,1)} async-done(((bf16[128,1024]{1,0:T(8,128)(2,1)}), bf16[2048,1024]{1,0:T(8,128)(2,1)}) %all-gather.10.cloned.1.call-update) | async-done | bytes 4194320 | tf_op jit(solution)/shard_map/all_gather | solution.py:93
  100.5 6.6 %fusion.26 = bf16[2,384,1024]{2,1,0:T(8,128)(2,1)S(1)} fusion(bf16[2048,1024]{1,0:T(8,128)(2,1)} %all-gather.10.cloned.1.call-done, bf16[2,384,2048]{2,1,0:T(8,128)(2,1)} %all-gather.8.cloned.1.call-done, f32[2048]{0:T(1024)S(1)} %copy-done.36, f32[2,384]{1,0:T(2,128)S(1)} %add_rsqrt_fusion), kind=kOutput, calls=%fused_computation.42 | convolution fusion | flops 3228303360 | bytes 8924160 | tf_op jit(solution)/shard_map/dot_general | solution.py:91
  107.2 3.1 collective-permute-start
  110.3 67.3 %all-gather.14.cloned.1.call-done = bf16[2048,1024]{1,0:T(8,128)(2,1)} async-done(((bf16[128,1024]{1,0:T(8,128)(2,1)}), bf16[2048,1024]{1,0:T(8,128)(2,1)}) %all-gather.14.cloned.1.call-update) | async-done | bytes 4194320 | tf_op jit(solution)/shard_map/all_gather | solution.py:98
  177.5 6.6 %fusion.31 = bf16[2,384,1024]{2,1,0:T(8,128)(2,1)S(1)} fusion(bf16[2048,1024]{1,0:T(8,128)(2,1)} %all-gather.14.cloned.1.call-done, bf16[2,384,2048]{2,1,0:T(8,128)(2,1)} %all-gather.8.cloned.1.call-done, f32[2048]{0:T(1024)S(1)} %copy-done.36, f32[2,384]{1,0:T(2,128)S(1)} %add_rsqrt_fusion), kind=kOutput, calls=%fused_computation.43 | convolution fusion | flops 3228303360 | bytes 8924160 | tf_op jit(solution)/shard_map/dot_general | solution.py:96
  184.8 3.1 collective-permute-start.1
  191.2 2.7 divide_bitcast_fusion.1
  194.0 3.2 copy.35
  197.2 3.1 div.39
  200.3 2.6 divide_bitcast_fusion
  202.9 2.8 copy.38
  205.7 5.4 %div.41 = f32[2,384,1024]{2,1,0:T(8,128)} reshape(f32[2,384,4,256]{3,2,1,0:T(4,128)} %copy.38) | data formatting | bytes 6291456 | tf_op jit(solution)/shard_map/div | solution.py:119
  211.1 7.8 %fusion.47 = (f32[2,384,1024]{2,1,0:T(8,128)}, f32[2,384,1024]{2,1,0:T(8,128)}) fusion(f32[2,384,1024]{2,1,0:T(8,128)} %param.24, f32[2,384,1024]{2,1,0:T(8,128)} %div.39, f32[1024]{0:T(1024)S(1)} %exponential_multiply_fusion, f32[2,384,1024]{2,1,0:T(8,128)} %div.41, f32[1024]{0:T(1024)S(1)} %bitcast.84, f32[2,387,1024]{2,1,0:T(8,128)S(1)} %copy-done.3, ...), kind=kLoop, calls=%fused_computation.62 | loop fusion | flops 11796480 | bytes 28332032 | tf_op jit(solution)/shard_map/exp | solution.py:123
  218.9 7.7 %slice.313 = f32[2,192,1024]{2,1,0:T(8,128)} slice(f32[2,384,1024]{2,1,0:T(8,128)} %get-tuple-element.59), slice={[0:2:1], [0:383:2], [0:1024:1]} | slice | bytes 3145728 | tf_op jit(solution)/shard_map/slice | solution.py:125
  226.7 4.2 slice.314
  230.8 7.6 %slice.352 = f32[2,192,1024]{2,1,0:T(8,128)} slice(f32[2,384,1024]{2,1,0:T(8,128)} %get-tuple-element.60), slice={[0:2:1], [0:383:2], [0:1024:1]} | slice | bytes 3145728 | tf_op jit(solution)/shard_map/slice | solution.py:125
  238.5 7.6 %slice.353 = f32[2,192,1024]{2,1,0:T(8,128)} slice(f32[2,384,1024]{2,1,0:T(8,128)} %get-tuple-element.60), slice={[0:2:1], [1:384:2], [0:1024:1]} | slice | bytes 3145728 | tf_op jit(solution)/shard_map/slice | solution.py:125
  246.1 5.5 %fusion.66 = (f32[2,192,1024]{2,1,0:T(8,128)}, f32[2,192,1024]{2,1,0:T(8,128)}) fusion(f32[2,192,1024]{2,1,0:T(8,128)} %slice.313, f32[2,192,1024]{2,1,0:T(8,128)} %slice.314, f32[2,192,1024]{2,1,0:T(8,128)} %slice.353, f32[2,192,1024]{2,1,0:T(8,128)} %slice.352), kind=kLoop, calls=%fused_computation.141 | loop fusion | flops 1179648 | bytes 9437184 | tf_op jit(solution)/shard_map/mul | solution.py:45
  251.6 4.3 slice.316
  255.9 4.3 slice.317
  260.2 4.3 slice.355
  264.5 4.3 slice.356
  268.9 3.4 fusion.67
  279.6 2.2 fusion.68
  286.6 2.0 fusion.69
  338.2 4.4 slice.347
  342.6 4.4 slice.386
  349.9 4.3 slice.349
  354.2 7.7 %slice.388 = f32[2,191,1024]{2,1,0:T(8,128)} slice(f32[2,384,1024]{2,1,0:T(8,128)} %get-tuple-element.60), slice={[0:2:1], [2:384:2], [0:1024:1]} | slice | bytes 3129344 | tf_op jit(solution)/shard_map/slice | solution.py:125
  380.2 6.2 %pad.129 = f32[2,384,1024]{2,1,0:T(8,128)} pad(f32[2,192,1024]{2,1,0:T(8,128)} %add.342, f32[]{:T(128)} %constant.70.clone.1), padding=0_0_0x1_0_1x0_0_0 | pad | bytes 4718596 | tf_op jit(solution)/shard_map/pad | solution.py:125
  386.4 2.1 pad_maximum_fusion.2
  388.5 3.5 pad.110
  391.9 3.4 pad.111
  395.4 3.5 add.317
  398.9 3.7 add_multiply_fusion.1
  404.0 6.6 %pad.128 = f32[2,384,1024]{2,1,0:T(8,128)} pad(f32[2,192,1024]{2,1,0:T(8,128)} %pad_maximum_fusion.1, f32[]{:T(128)} %constant.70.clone.1), padding=0_0_0x0_1_1x0_0_0 | pad | bytes 4718596 | tf_op jit(solution)/shard_map/pad | solution.py:125
  411.4 8.5 %all-gather.1 = f32[8,1,1024]{2,1,0:T(1,128)S(1)} all-gather(f32[2,1,1024]{2,1,0:T(1,128)S(1)} %slice_add_fusion.3), channel_id=3, replica_groups=mesh['sp'=4,'fs'=4,'tp'=2] {'sp'}, dimensions={0}, use_global_device_ids=true | all-gather | bytes 40960 | tf_op jit(solution)/shard_map/all_gather | solution.py:21
  420.0 6.2 %pad.113 = f32[2,384,1024]{2,1,0:T(8,128)} pad(f32[2,192,1024]{2,1,0:T(8,128)} %add.317, f32[]{:T(128)} %constant.70.clone.1), padding=0_0_0x1_0_1x0_0_0 | pad | bytes 4718596 | tf_op jit(solution)/shard_map/pad | solution.py:125
  426.2 2.9 pad_maximum_fusion
  429.0 6.2 %pad.112 = f32[2,384,1024]{2,1,0:T(8,128)} pad(f32[2,192,1024]{2,1,0:T(8,128)} %pad_maximum_fusion, f32[]{:T(128)} %constant.70.clone.1), padding=0_0_0x0_1_1x0_0_0 | pad | bytes 4718596 | tf_op jit(solution)/shard_map/pad | solution.py:125
  436.1 10.3 %all-gather = f32[8,1,1024]{2,1,0:T(1,128)S(1)} all-gather(f32[2,1,1024]{2,1,0:T(1,128)S(1)} %slice_add_fusion.6), channel_id=2, replica_groups=mesh['sp'=4,'fs'=4,'tp'=2] {'sp'}, dimensions={0}, use_global_device_ids=true | all-gather | bytes 40960 | tf_op jit(solution)/shard_map/all_gather | solution.py:21
  451.9 2.1 fusion.23
  456.8 8.8 %fusion.3 = f32[384,2,2048]{2,0,1:T(8,128)} fusion(bf16[1024,2048]{1,0:T(8,128)(2,1)} %all-gather.16.cloned.1.call-done, bf16[2,384,1024]{1,2,0:T(8,128)(2,1)} %fusion.22), kind=kOutput, calls=%fused_computation.9 | convolution fusion | flops 3221225472 | bytes 12058624 | tf_op jit(solution)/shard_map/dot_general | solution.py:156
  465.5 12.9 %fusion.11 = f32[384,2,2048]{2,0,1:T(8,128)} fusion(f32[384,2,2048]{2,0,1:T(8,128)} %fusion.3, bf16[1024,2048]{1,0:T(8,128)(2,1)} %all-gather.12.cloned.1.call-done, f32[2,384,1024]{2,1,0:T(8,128)} %pad.128, f32[2,384,1024]{2,1,0:T(8,128)S(1)} %copy-done.7, f32[2,384,1024]{2,1,0:T(8,128)} %pad.112, f32[2,384,1024]{2,1,0:T(8,128)} %pad.113, ...), kind=kOutput, calls=%fused_computation.17 | convolution fusion | flops 3226730496 | bytes 29368320 | tf_op jit(solution)/shard_map/dot_general | solution.py:155
  478.5 21.9 %reduce-scatter.2.cloned.1.call-done = f32[192,2,2048]{2,0,1:T(8,128)} async-done(((f32[384,2,2048]{2,0,1:T(8,128)}), f32[192,2,2048]{2,0,1:T(8,128)}) %reduce-scatter.2.cloned.1.call-update) | async-done | bytes 3145744 | tf_op jit(solution)/shard_map/reduce_scatter | solution.py:154
  500.4 3.3 convert_bitcast_fusion
  (223 shorter events, 105.2 us)
Async XLA Ops:
  6.5 184.7 %copy-start = (bf16[4,256,256]{2,1,0:T(8,128)(2,1)S(1)}, bf16[4,256,256]{2,1,0:T(8,128)(2,1)}, u32[]{:S(2)}) copy-start(bf16[4,256,256]{2,1,0:T(8,128)(2,1)} %param.21) | copy-start | bytes 1572868
  6.5 16.3 %all-gather.8.cloned.1.call-start = ((), (), s32[]{:S(2)}) async-start(), calls=%async_computation.1 | async-start | bytes 4718592 | tf_op jit(solution)/shard_map/all_gather | solution.py:80
  7.3 93.3 %copy-start.36 = (f32[2048]{0:T(1024)S(1)}, f32[2048]{0:T(1024)}, u32[]{:S(2)}) copy-start(f32[2048]{0:T(1024)} %param.17) | copy-start | bytes 24580
  7.3 93.3 %all-gather.10.cloned.1.call-start = ((), (), s32[]{:S(2)}) async-start(), calls=%async_computation.2 | async-start | bytes 4456448 | tf_op jit(solution)/shard_map/all_gather | solution.py:93
  8.0 169.5 %all-gather.14.cloned.1.call-start = ((), (), s32[]{:S(2)}) async-start(), calls=%async_computation.4 | async-start | bytes 4456448 | tf_op jit(solution)/shard_map/all_gather | solution.py:98
  8.8 448.0 %all-gather.16.cloned.1.call-start = ((), (), s32[]{:S(2)}) async-start(), calls=%async_computation.5 | async-start | bytes 4456448 | tf_op jit(solution)/shard_map/all_gather | solution.py:152
  9.3 456.2 %all-gather.12.cloned.1.call-start = ((), (), s32[]{:S(2)}) async-start(), calls=%async_computation.3 | async-start | bytes 4456448 | tf_op jit(solution)/shard_map/all_gather | solution.py:151
  9.9 490.4 %reduce-scatter.2.cloned.1.call-start = ((), (), s32[]{:S(2)}) async-start(), calls=%async_computation.6 | async-start | bytes 9437184 | tf_op jit(solution)/shard_map/reduce_scatter | solution.py:154
  107.2 80.8 %collective-permute-start = (bf16[2,3,1024]{2,1,0:T(4,128)(2,1)S(1)}, bf16[2,3,1024]{2,1,0:T(4,128)(2,1)S(1)}, u32[]{:S(2)}, u32[]{:S(2)}) collective-permute-start(bf16[2,3,1024]{2,1,0:T(4,128)(2,1)S(1)} %slice.401), channel_id=1, source_target_pairs={{0,8},{8,16},{16,24},{1,9},{9,17},{17,25},{2,10},{10,18},{18,26},{... | collective-permute-start | bytes 36872 | tf_op jit(solution)/shard_map/ppermute | solution.py:16
  184.1 3.8 copy-start.8
  184.8 261.8 %collective-permute-start.1 = (bf16[2,15,1024]{2,1,0:T(8,128)(2,1)}, bf16[2,15,1024]{2,1,0:T(8,128)(2,1)}, u32[]{:S(2)}, u32[]{:S(2)}) collective-permute-start(bf16[2,15,1024]{2,1,0:T(8,128)(2,1)} %slice.458), channel_id=1, source_target_pairs={{0,8},{8,16},{16,24},{1,9},{9,17},{17,25},{2,10},{10,18},{18,26},{... | collective-permute-start | bytes 184328 | tf_op jit(solution)/shard_map/ppermute | solution.py:16
  188.4 1.6 copy-start.2
  190.1 1.2 copy-start.15
  205.7 5.4 %copy-start.3 = (f32[2,387,1024]{2,1,0:T(8,128)S(1)}, f32[2,387,1024]{2,1,0:T(8,128)}, u32[]{:S(2)}) copy-start(f32[2,387,1024]{2,1,0:T(8,128)} %copy-done.2) | copy-start | bytes 9510916
  218.9 7.8 %copy-start.4 = (f32[2,384,1024]{2,1,0:T(8,128)S(1)}, f32[2,384,1024]{2,1,0:T(8,128)}, u32[]{:S(2)}) copy-start(f32[2,384,1024]{2,1,0:T(8,128)} %get-tuple-element.59) | copy-start | bytes 9437188
  363.9 5.5 %copy-start.19 = (f32[2,11,1024]{2,1,0:T(8,128)S(1)}, f32[2,11,1024]{2,1,0:T(8,128)}, u32[]{:S(2)}) copy-start(f32[2,11,1024]{2,1,0:T(8,128)} %slice.341) | copy-start | bytes 270340
  363.9 5.5 %copy-start.20 = (f32[2,11,1024]{2,1,0:T(8,128)S(1)}, f32[2,11,1024]{2,1,0:T(8,128)}, u32[]{:S(2)}) copy-start(f32[2,11,1024]{2,1,0:T(8,128)} %slice.380) | copy-start | bytes 270340
  363.9 5.5 %copy-start.30 = (f32[2,1,1024]{2,1,0:T(1,128)S(1)}, f32[2,1,1024]{2,1,0:T(1,128)}, u32[]{:S(2)}) copy-start(f32[2,1,1024]{2,1,0:T(1,128)} %slice.436) | copy-start | bytes 24580
  363.9 5.8 %copy-start.29 = (f32[2,1,1024]{2,1,0:T(1,128)S(1)}, f32[2,1,1024]{2,1,0:T(1,128)}, u32[]{:S(2)}) copy-start(f32[2,1,1024]{2,1,0:T(1,128)} %slice.410) | copy-start | bytes 24580
  366.7 3.1 copy-start.16
  366.7 3.1 copy-start.17
  369.3 0.7 copy-start.28
  369.5 0.8 copy-start.27
  370.0 1.4 copy-start.14
  370.4 1.2 copy-start.26
  371.4 1.8 copy-start.25
  373.4 2.0 copy-start.12
  373.4 2.0 copy-start.13
  375.4 1.4 copy-start.24
  380.2 6.2 %copy-start.23 = (f32[2,1,1024]{2,1,0:T(1,128)S(1)}, f32[2,1,1024]{2,1,0:T(1,128)}, u32[]{:S(2)}) copy-start(f32[2,1,1024]{2,1,0:T(1,128)} %slice.407) | copy-start | bytes 24580
  395.4 3.6 copy-start.5
  395.4 3.6 copy-start.6
  395.4 3.6 copy-start.11
  398.9 3.7 copy-start.22
  404.0 6.6 %copy-start.7 = (f32[2,384,1024]{2,1,0:T(8,128)S(1)}, f32[2,384,1024]{2,1,0:T(8,128)}, u32[]{:S(2)}) copy-start(f32[2,384,1024]{2,1,0:T(8,128)} %pad.129) | copy-start | bytes 9437188
  410.5 15.6 %copy-start.21 = (f32[2,1,1024]{2,1,0:T(1,128)S(1)}, f32[2,1,1024]{2,1,0:T(1,128)}, u32[]{:S(2)}) copy-start(f32[2,1,1024]{2,1,0:T(1,128)} %slice.406) | copy-start | bytes 24580
  429.0 17.6 %copy-start.31 = (f32[2,1024]{1,0:T(2,128)S(1)}, f32[2,1024]{1,0:T(2,128)}, u32[]{:S(2)}) copy-start(f32[2,1024]{1,0:T(2,128)} %param.25) | copy-start | bytes 24580
  450.0 1.4 copy-start.9
  450.0 1.9 copy-start.10
  450.0 1.9 copy-start.32
  450.0 1.9 copy-start.33
  450.0 1.9 copy-start.35
  451.9 2.1 copy-start.18
  454.6 0.7 copy-start.34
  478.4 25.2 %copy-start.1 = (bf16[4,256,256]{2,1,0:T(8,128)(2,1)S(1)}, bf16[4,256,256]{2,1,0:T(8,128)(2,1)}, u32[]{:S(2)}) copy-start(bf16[4,256,256]{2,1,0:T(8,128)(2,1)} %param.21) | copy-start | bytes 1572868
Sparse Core Ops, SparseCore 0:
  8.9 13.9 all-gather.7
  25.6 74.8 all-gather.9
  103.3 74.1 all-gather.13
  180.1 85.2 all-gather.15
  267.9 86.8 all-gather.11
  478.6 21.7 reduce-scatter.1
where the time goes:
time: 516 us; the launch traced here: 510 us
  local copies, waits for them, and re-layouts  184 us (36%)
  waiting for transfers between devices  176 us (34%)
  other arithmetic  70.5 us (14%)
  matrix products  40.8 us (8%)
  blocking collectives  18.7 us (4%)
  between operations  14.3 us (3%)
  starting transfers between devices  6.37 us (1%)
    slice x56, local copies, waits for them, and re-layouts, per_device(): lax.associative_scan(combine, (decay_factor, drive_term), axis=1)  128 us
    all_gather x1, waiting for transfers between devices, per_device(): lax.all_gather(chain_entry, ('sp', 'fs'), axis=0, tiled=True)  75 us
    all_gather x1, waiting for transfers between devices, per_device(): lax.all_gather(pool_entry, ('sp', 'fs'), axis=0, tiled=True)  67.3 us
    pad x30, local copies, waits for them, and re-layouts, per_device(): lax.associative_scan(combine, (decay_factor, drive_term), axis=1)  36.5 us
    mul x15, other arithmetic, combine(): return (earlier[0] * latter[0], latter[0] * earlier[1] + latter[1])  24.6 us
    reduce_scatter x1, waiting for transfers between devices, per_device(): lax.psum_scatter(jnp.dot(recurrent_rows, full_chain, preferred_element_ty...  21.9 us
    all_gather x2, blocking collectives, carried_in(): gathered = jax.tree.map(lambda a: lax.all_gather(a, axis), part)  18.7 us
    div x4, local copies, waits for them, and re-layouts, per_device(): gate_recur = jax.nn.sigmoid(block_map(conv_out, recur_gate))  14.5 us
  transfers between devices with their start and end apart: 8, of which 4 were waited for; matrix products, arithmetic and copies ran while one was open for 54% of the time, Pallas kernels for 0%

commit v1 on v0

v1 whole, which is shorter than its diff:
```python
import functools

import jax
import jax.numpy as jnp
from jax import lax
from jax.experimental import pallas as pl
from jax.experimental.pallas import tpu as pltpu
from jax.sharding import PartitionSpec as P

MESH = pl.DeviceIdType.MESH
NORM_EPSILON = 1e-06
RECUR_SCALE = 8.0
HALO = 16
COLS = 256
ROWS = 64
F32 = jnp.float32
BF16 = jnp.bfloat16


def neg_expm1(x):
    y = -x
    poly = 1.0 - y * (1.0 / 9.0)
    for k in range(8, 1, -1):
        poly = 1.0 - y * (1.0 / k) * poly
    return jnp.where(y < 0.5, y * poly, 1.0 - jnp.exp(x))


def kernel(
    n, m,
    tokens, gain, chain_entry, pool_entry, taps, rgate, igate, dlog, shift_hbm, start,
    pmix, pscale, chain_exit, pool_exit,
    out,
    w0, w1, w2, w3, raw, normed, cbuf, pbuf, shift, rg, ig, pm,
    convb, zr, zi, cum_a, cum_b, rec, pooled, my_ab, all_ab, ent, acc, sendbuf, recvbuf,
    s1, r1, s2, r2, loc, nsem, hsem_s, hsem_r, ab_s, ab_r, out_s, out_r,
):
    sp, fs, tp = lax.axis_index("sp"), lax.axis_index("fs"), lax.axis_index("tp")
    shards = (chain_entry, pool_entry, chain_exit, pool_exit)
    bufs = (w0, w1, w2, w3)
    seqs, half_rows, width = raw.shape
    rows = 2 * half_rows
    chans = cbuf.shape[2]
    nb = chans // COLS
    far = m // 2
    full = (m - 1) // 2

    def ring(i):
        return i + (i // 2) * (5 - 2 * i) if m == 4 else i

    pos = ring(fs)
    right, left = ring((pos + 1) % m), ring((pos + m - 1) % m)

    barrier = pltpu.get_barrier_semaphore()
    greet = [{"sp": (sp + k) % n} for k in range(1, n)] + [{"tp": 1 - tp}]
    if m > 1:
        greet += [{"fs": right}, {"fs": left}]
    for device in greet:
        pl.semaphore_signal(barrier, inc=1, device_id=device, device_id_type=MESH)

    def region(w, p, q, part=None):
        block = shards[w].shape[0]
        at = (((sp + p) % n) * m + ring((pos + q + m) % m)) * block
        if part is None:
            return bufs[w].at[pl.ds(pl.multiple_of(at, block), block)]
        half = block // 2
        return bufs[w].at[pl.ds(pl.multiple_of(at + part * half, half), half)]

    started = []

    def launch(copy):
        copy.start()
        started.append(copy)

    def first(w, k):
        return pltpu.make_async_remote_copy(
            src_ref=shards[w], dst_ref=region(w, 0, 0), send_sem=s1.at[w * n + k],
            recv_sem=r1.at[w * n + n - k], device_id={"sp": (sp + k) % n}, device_id_type=MESH)

    def first_wait(w, p):
        pltpu.make_async_remote_copy(
            src_ref=shards[w], dst_ref=region(w, p, 0), send_sem=s1.at[w * n + p],
            recv_sem=r1.at[w * n + p], device_id={"sp": (sp + p) % n},
            device_id_type=MESH).wait_recv()

    def second(w, p, way, d):
        q = -d if way == 0 else d
        part = way if (m % 2 == 0 and d + 1 == far) else None
        if p == 0 and d == 0:
            src = shards[w]
            if part is not None:
                half = shards[w].shape[0] // 2
                src = src.at[pl.ds(part * half, half)]
        else:
            src = region(w, p, q, part)
        at = ((w * n + p) * 2 + way) * max(far, 1) + d
        return pltpu.make_async_remote_copy(
            src_ref=src, dst_ref=region(w, p, q, part), send_sem=s2.at[at], recv_sem=r2.at[at],
            device_id={"fs": right if way == 0 else left}, device_id_type=MESH)

    def second_wait(w, p, way, d):
        q = -d if way == 0 else d
        part = way if (m % 2 == 0 and d == far) else None
        at = ((w * n + p) * 2 + way) * max(far, 1) + d - 1
        ref = region(w, p, q, part)
        pltpu.make_async_remote_copy(
            src_ref=ref, dst_ref=ref, send_sem=s2.at[at], recv_sem=r2.at[at],
            device_id={"fs": right if way == 0 else left}, device_id_type=MESH).wait_recv()

    def second_all(w, p):
        if far >= 1:
            for way in (0, 1):
                launch(second(w, p, way, 0))

    def forward(w, p):
        for d in range(1, far):
            for way in (0, 1):
                second_wait(w, p, way, d)
                launch(second(w, p, way, d))

    def last_wait(w, p):
        if far >= 1:
            for way in (0, 1):
                second_wait(w, p, way, far)

    local = [
        pltpu.make_async_copy(tokens, raw, loc.at[0]),
        pltpu.make_async_copy(shift_hbm, shift, loc.at[1]),
        pltpu.make_async_copy(rgate, rg, loc.at[2]),
        pltpu.make_async_copy(igate, ig, loc.at[3]),
        pltpu.make_async_copy(pmix, pm, loc.at[4]),
    ] + [pltpu.make_async_copy(shards[w], region(w, 0, 0), loc.at[5 + w]) for w in range(4)]
    for copy in local:
        copy.start()

    pl.semaphore_wait(barrier, len(greet))
    order = sorted(range(1, n), key=lambda p: min(p, n - p))
    for w in (0, 1):
        second_all(w, 0)
        for k in order:
            launch(first(w, k))

    local[0].wait()
    mine = tp * half_rows

    def norm_step(i, c):
        s, r = i // (half_rows // ROWS), (i % (half_rows // ROWS)) * ROWS
        x = raw[s, pl.ds(pl.multiple_of(r, ROWS), ROWS), :].astype(F32)
        scale = lax.rsqrt(jnp.mean(x * x, axis=-1, keepdims=True) + NORM_EPSILON)
        normed[s, pl.ds(pl.multiple_of(mine + r, ROWS), ROWS), :] = (
            x * scale * gain[...]).astype(BF16)
        return c

    lax.fori_loop(0, seqs * (half_rows // ROWS), norm_step, 0)

    def normed_copy(owner):
        ref = normed.at[:, pl.ds(pl.multiple_of(owner * half_rows, ROWS), half_rows)]
        return pltpu.make_async_remote_copy(
            src_ref=ref, dst_ref=ref, send_sem=nsem.at[0], recv_sem=nsem.at[1],
            device_id={"tp": 1 - tp}, device_id_type=MESH)

    for p in order:
        for w in (0, 1):
            first_wait(w, p)
            second_all(w, p)
        if p == order[0]:
            launch(normed_copy(tp))
    for w in (2, 3):
        for k in order:
            launch(first(w, k))
    for p in [0] + order:
        for w in (0, 1):
            forward(w, p)
    for w in (2, 3):
        second_all(w, 0)
    for p in [0] + order:
        for w in (0, 1):
            last_wait(w, p)
    for p in order:
        for w in (2, 3):
            first_wait(w, p)
            second_all(w, p)
    for copy in local[1:]:
        copy.wait()
    normed_copy(1 - tp).wait_recv()

    def lanes(c):
        return pl.ds(pl.multiple_of(c * COLS, COLS), COLS)

    def entry_step(i, c):
        s, b = i // nb, lanes(i % nb)
        x = normed[s]
        cbuf[s, HALO:, b] = jnp.dot(x, w0[:, b], preferred_element_type=F32).astype(BF16)
        pbuf[s, HALO:, b] = jnp.dot(x, w1[:, b], preferred_element_type=F32).astype(BF16)
        return c

    lax.fori_loop(0, seqs * nb, entry_step, 0)

    def halo(i, ref):
        return pltpu.make_async_remote_copy(
            src_ref=ref.at[:, rows:], dst_ref=ref.at[:, :HALO], send_sem=hsem_s.at[i],
            recv_sem=hsem_r.at[i], device_id={"sp": (sp + 1) % n}, device_id_type=MESH)

    todo = [(w, p) for p in [0] + order for w in (2, 3)]

    def some_forwards(count):
        for w, p in todo[:count]:
            forward(w, p)
        del todo[:count]

    some_forwards(2)

    @pl.when(sp < n - 1)
    def _():
        halo(0, cbuf).start()
        halo(1, pbuf).start()

    @pl.when(sp > 0)
    def _():
        halo(0, cbuf).wait_recv()
        halo(1, pbuf).wait_recv()

    @pl.when(sp == 0)
    def _():
        cbuf[:, :HALO, :] = jnp.zeros((seqs, HALO, chans), BF16)
        pbuf[:, :HALO, :] = jnp.zeros((seqs, HALO, chans), BF16)

    tap_count = taps.shape[0]
    inverse_length = 1.0 / (rows * n)

    def chain_step(g, s):
        b = lanes(g)
        tap = taps[:, b].astype(F32)

        def conv(i, c):
            r = pl.multiple_of(i * ROWS, ROWS)
            v = cbuf[s, pl.ds(r, ROWS + HALO), b].astype(F32)
            total = v * tap[tap_count - 1 : tap_count]
            for j in range(tap_count - 1):
                total = total + pltpu.roll(v, tap_count - 1 - j, 0) * tap[j : j + 1]
            convb[pl.ds(r, ROWS), :] = total[HALO:].astype(BF16)
            return c

        lax.fori_loop(0, rows // ROWS, conv, 0)
        x = convb[...]
        zr[...] = jnp.dot(x, rg[g], preferred_element_type=F32)
        zi[...] = jnp.dot(x, ig[g], preferred_element_type=F32)
        rate = -RECUR_SCALE * (jnp.exp(dlog[:, b]) * inverse_length)
        row = lax.broadcasted_iota(jnp.int32, (ROWS, COLS), 0)

        def scan(i, carry):
            r = pl.multiple_of(i * ROWS, ROWS)
            at = pl.ds(r, ROWS)
            log_decay = jax.nn.sigmoid(zr[at, :]) * rate + shift[s, at, b]
            a = jnp.exp(log_decay)
            d = (jnp.sqrt(neg_expm1(2.0 * log_decay)) * jax.nn.sigmoid(zi[at, :])
                 * convb[at, :].astype(F32))
            k = 1
            while k < ROWS:
                before = row >= k
                d = d + a * jnp.where(before, pltpu.roll(d, k, 0), 0.0)
                a = a * jnp.where(before, pltpu.roll(a, k, 0), 1.0)
                k *= 2
            d = d + a * carry[1]
            a = a * carry[0]
            cum_a[s, at, b] = a
            cum_b[s, at, b] = d
            return a[ROWS - 1 :], d[ROWS - 1 :]

        end = lax.fori_loop(
            0, rows // ROWS, scan, (jnp.ones((1, COLS), F32), jnp.zeros((1, COLS), F32)))
        my_ab[pl.ds(s, 1), b] = end[0]
        my_ab[pl.ds(seqs + s, 1), b] = end[1]

    for s in range(seqs):
        def chain_group(g, c, s=s):
            chain_step(g, s)
            return c

        for g0 in range(0, nb, 2):
            lax.fori_loop(g0, min(g0 + 2, nb), chain_group, 0)
            some_forwards(max(1, len(todo) // (2 * seqs)))

    def ab_copy(k):
        return pltpu.make_async_remote_copy(
            src_ref=my_ab, dst_ref=all_ab.at[k], send_sem=ab_s.at[k], recv_sem=ab_r.at[k],
            device_id={"sp": (sp + k) % n}, device_id_type=MESH)

    def pool_group(g):
        b = slice(g * COLS, (g + 1) * COLS)
        window = 2 ** (1 + g % 4)

        def diff(i, c):
            s, r = i // (rows // ROWS), pl.multiple_of((i % (rows // ROWS)) * ROWS, ROWS)
            v = pbuf[s, pl.ds(r, ROWS + HALO), b].astype(F32)
            total, k = v, 1
            while k < window:
                total = total + pltpu.roll(total, k, 0)
                k *= 2
            t = lax.broadcasted_iota(jnp.int32, (ROWS, COLS), 0) + (sp * rows + r + 1)
            count = jnp.minimum(t, window).astype(F32)
            convb_pool = total[HALO:] / count - v[HALO:]
            pooled[s, pl.ds(r, ROWS), b] = convb_pool.astype(BF16)
            return c

        lax.fori_loop(0, seqs * (rows // ROWS), diff, 0)
        for s in range(seqs):
            y = jnp.dot(pooled[s, :, b], pm[g], preferred_element_type=F32)
            pooled[s, :, b] = (y * pscale[:, b]).astype(BF16)

    pool_group(0)
    for k in range(1, n):
        @pl.when(sp + k < n)
        def _(k=k):
            ab_copy(k).start()

    for g in range(1, nb):
        pool_group(g)
        some_forwards(1)
    some_forwards(len(todo))

    ent[...] = start[...]
    for k in range(n - 1, 0, -1):
        @pl.when(sp >= k)
        def _(k=k):
            ab_copy(k).wait_recv()
            ent[...] = all_ab[k, :seqs, :] * ent[...] + all_ab[k, seqs : 2 * seqs, :]

    for s in range(seqs):
        def fix(i, c, s=s):
            at = pl.ds(pl.multiple_of(i * ROWS, ROWS), ROWS)
            rec[s, at, :] = (cum_a[s, at, :] * ent[s : s + 1, :] + cum_b[s, at, :]).astype(BF16)
            return c

        lax.fori_loop(0, rows // ROWS, fix, 0)

    for p in [0] + order:
        for w in (2, 3):
            last_wait(w, p)

    out_count = width // COLS
    dims = (((1,), (1,)), ((), ()))

    def partial(owner, j):
        at = pl.ds(pl.multiple_of(owner * half_rows, ROWS), half_rows)
        b = lanes(j)
        x = rec[:, at, :].reshape(seqs * half_rows, chans)
        y = pooled[:, at, :].reshape(seqs * half_rows, chans)
        return lax.dot_general(x, w2[b, :], dims, preferred_element_type=F32) + lax.dot_general(
            y, w3[b, :], dims, preferred_element_type=F32)

    def out_copy(j):
        return pltpu.make_async_remote_copy(
            src_ref=sendbuf.at[j], dst_ref=recvbuf.at[j], send_sem=out_s.at[j],
            recv_sem=out_r.at[j], device_id={"tp": 1 - tp}, device_id_type=MESH)

    def exit_step(j, c):
        sendbuf[j] = partial(1 - tp, j).astype(BF16)
        acc[j] = partial(tp, j)
        out_copy(j).start()
        return c

    lax.fori_loop(0, out_count, exit_step, 0)

    def out_step(j, c):
        out_copy(j).wait_recv()
        total = (acc[j] + recvbuf[j].astype(F32)).astype(BF16)
        out[:, :, lanes(j)] = total.reshape(seqs, half_rows, COLS)
        return c

    lax.fori_loop(0, out_count, out_step, 0)

    def out_end(j, c):
        out_copy(j).wait_send()
        return c

    lax.fori_loop(0, out_count, out_end, 0)
    for copy in started:
        copy.wait_send()

    @pl.when(sp < n - 1)
    def _():
        halo(0, cbuf).wait_send()
        halo(1, pbuf).wait_send()

    for k in range(1, n):
        @pl.when(sp + k < n)
        def _(k=k):
            ab_copy(k).wait_send()


def per_device(n, m, *args):
    (tokens, norm_gain, chain_entry, pool_entry, conv_taps, recur_gate, input_gate, decay_log,
     decay_shift, start_state, pool_mix, pool_scale, chain_exit, pool_exit) = args
    seqs, half_rows, width = tokens.shape
    rows, chans = 2 * half_rows, chain_entry.shape[1]
    nb = chans // COLS
    assert pool_mix.shape[0] % 4 == 0 and pool_mix.shape[1] == COLS
    far = max(m // 2, 1)
    hbm, vmem = pl.BlockSpec(memory_space=pl.ANY), pl.BlockSpec(memory_space=pltpu.VMEM)
    dma = pltpu.SemaphoreType.DMA
    ab_rows = -(-2 * seqs // 8) * 8
    out_count = width // COLS
    scratch = [pltpu.VMEM((width, chans), BF16)] * 4 + [
        pltpu.VMEM((seqs, half_rows, width), BF16),
        pltpu.VMEM((seqs, rows, width), BF16),
        pltpu.VMEM((seqs, HALO + rows, chans), BF16),
        pltpu.VMEM((seqs, HALO + rows, chans), BF16),
        pltpu.VMEM((seqs, rows, chans), F32),
        pltpu.VMEM(recur_gate.shape, BF16),
        pltpu.VMEM(input_gate.shape, BF16),
        pltpu.VMEM(pool_mix.shape, BF16),
        pltpu.VMEM((rows, COLS), BF16),
        pltpu.VMEM((rows, COLS), F32),
        pltpu.VMEM((rows, COLS), F32),
        pltpu.VMEM((seqs, rows, chans), F32),
        pltpu.VMEM((seqs, rows, chans), F32),
        pltpu.VMEM((seqs, rows, chans), BF16),
        pltpu.VMEM((seqs, rows, chans), BF16),
        pltpu.VMEM((ab_rows, chans), F32),
        pltpu.VMEM((n, ab_rows, chans), F32),
        pltpu.VMEM((seqs, chans), F32),
        pltpu.VMEM((out_count, seqs * half_rows, COLS), F32),
        pltpu.VMEM((out_count, seqs * half_rows, COLS), BF16),
        pltpu.VMEM((out_count, seqs * half_rows, COLS), BF16),
        dma((4 * n,)), dma((4 * n,)), dma((8 * n * far,)), dma((8 * n * far,)),
        dma((9,)), dma((2,)), dma((2,)), dma((2,)), dma((n,)), dma((n,)),
        dma((out_count,)), dma((out_count,)),
    ]
    return pl.pallas_call(
        functools.partial(kernel, n, m),
        name="layer",
        out_shape=jax.ShapeDtypeStruct(tokens.shape, BF16),
        in_specs=[hbm, vmem, hbm, hbm, vmem, hbm, hbm, vmem, hbm, vmem, hbm, vmem, hbm, hbm],
        out_specs=vmem,
        scratch_shapes=scratch,
        compiler_params=pltpu.CompilerParams(
            collective_id=0, has_side_effects=True, vmem_limit_bytes=62 * 1024 * 1024),
    )(tokens, norm_gain[None], chain_entry, pool_entry, conv_taps, recur_gate, input_gate,
      decay_log[None], decay_shift, start_state, pool_mix, pool_scale[None],
      chain_exit.T, pool_exit.T)


def solution(mesh):
    in_specs = (
        P("fs", ("sp", "tp"), None),
        P(),
        P(("sp", "fs"), "tp"),
        P(("sp", "fs"), "tp"),
        P(None, "tp"),
        P("tp", None, None),
        P("tp", None, None),
        P("tp"),
        P("fs", "sp", "tp"),
        P("fs", "tp"),
        P("tp", None, None),
        P("tp"),
        P("tp", ("sp", "fs")),
        P("tp", ("sp", "fs")),
    )
    out_specs = P("fs", ("sp", "tp"), None)
    return jax.shard_map(
        functools.partial(per_device, mesh.shape["sp"], mesh.shape["fs"]),
        mesh=mesh, in_specs=in_specs, out_specs=out_specs, check_vma=False)
```

time: 516 us -> 183 us (0.35); the launches traced: 510 us -> 183 us
  local copies, waits for them, and re-layouts: 184 us -> 6.31 us
  Pallas kernels: 0 us -> 177 us
  waiting for transfers between devices: 176 us -> 0 us
  other arithmetic: 70.5 us -> 0 us
  matrix products: 40.8 us -> 0 us
  blocking collectives: 18.7 us -> 0 us
  between operations: 14.3 us -> 0.01 us
  starting transfers between devices: 6.37 us -> 0 us
    pallas_call x0 -> x1, Pallas kernels: none -> 177 us  [per_device(): pl.pallas_call(functools.partial(kernel, n, m), name='layer', out_shape=j...]
    all_gather x5 -> x0, waiting for transfers between devices: 151 us -> none  [the longest x1 75 us: per_device(): lax.all_gather(chain_entry, ('sp', 'fs'), axis=0, tiled=True)]
    slice x58 -> x0, local copies, waits for them, and re-layouts: 129 us -> none  [the longest x56 128 us: per_device(): lax.associative_scan(combine, (decay_factor, drive_term), axis=1)]
    dot_general x7 -> x0, matrix products: 40.8 us -> none  [the longest x1 12.9 us: per_device(): jnp.dot(recurrent_rows, full_chain, preferred_element_type=jnp.float32)]
    pad x30 -> x0, local copies, waits for them, and re-layouts: 36.5 us -> none  [per_device(): lax.associative_scan(combine, (decay_factor, drive_term), axis=1)]
    mul x16 -> x0, other arithmetic: 25.3 us -> none  [the longest x15 24.6 us: combine(): return (earlier[0] * latter[0], latter[0] * earlier[1] + latter[1])]
    reduce_scatter x1 -> x0, waiting for transfers between devices: 21.9 us -> none  [per_device(): lax.psum_scatter(jnp.dot(recurrent_rows, full_chain, preferred_element_ty...]
    all_gather x2 -> x0, blocking collectives: 18.7 us -> none  [carried_in(): gathered = jax.tree.map(lambda a: lax.all_gather(a, axis), part)]
  transfers between devices with their start and end apart: 8 -> 0, of which waited for: 4 -> 0; matrix products, arithmetic and copies ran while one was open for 54% -> 0% of each run, Pallas kernels for 0% -> 0%
where the time goes in v1:
time: 183 us
  Pallas kernels  177 us (97%)
  local copies, waits for them, and re-layouts  6.31 us (3%)
    pallas_call x1, Pallas kernels, per_device(): pl.pallas_call(functools.partial(kernel, n, m), name='layer', out_shape=j...  177 us
    unnamed x3, local copies, waits for them, and re-layouts  6.31 us

profile of v1, /device:TPU:11, one launch (start us, length us, event | category | flops | bytes accessed | tf_op | source)
XLA Modules:
  0.0 183.2 jit_solution(4867748078731026582)
XLA Ops:
  0.0 1.8 copy.15
  1.8 1.8 copy.16
  3.6 176.8 %layer.1 = bf16[2,192,2048]{2,1,0:T(8,128)(2,1)} custom-call(bf16[2,192,2048]{2,1,0:T(8,128)(2,1)} %tokens.1, f32[1,2048]{1,0:T(1,128)} %bitcast.7, bf16[128,1024]{1,0:T(8,128)(2,1)} %chain_entry.1, bf16[128,1024]{1,0:T(8,128)(2,1)} %pool_entry.1, bf16[4,1024]{1,0:T(4,128)(2,1)} %taps.1, bf16[4,256,256]{2,1,0:T(8,128)(2,1)} %rgate.1, ...), custom_call_target="tpu_custom_call" | custom-call | tf_op jit(solution)/shard_map/layer/pallas_call | solution.py:429
  180.4 2.7 %copy.18 = bf16[2,192,2048]{2,1,0:T(8,128)(2,1)} copy(bf16[2,192,2048]{2,1,0:T(8,128)(2,1)} %layer.1) | data formatting | bytes 3145728

commit v2 on v1

--- a/solution.py
+++ b/solution.py
@@ -32,7 +32,7 @@
     out,
     w0, w1, w2, w3, raw, normed, cbuf, pbuf, shift, rg, ig, pm,
     convb, zr, zi, cum_a, cum_b, rec, pooled, my_ab, all_ab, ent, acc, sendbuf, recvbuf,
-    s1, r1, s2, r2, loc, nsem, hsem_s, hsem_r, ab_s, ab_r, out_s, out_r,
+    s1, r1, s2, r2, t1s, t1r, t2s, t2r, loc, nsem, hsem_s, hsem_r, ab_s, ab_r, out_s, out_r,
 ):
     sp, fs, tp = lax.axis_index("sp"), lax.axis_index("fs"), lax.axis_index("tp")
     shards = (chain_entry, pool_entry, chain_exit, pool_exit)
@@ -52,18 +52,30 @@
 
     barrier = pltpu.get_barrier_semaphore()
     greet = [{"sp": (sp + k) % n} for k in range(1, n)] + [{"tp": 1 - tp}]
-    if m > 1:
-        greet += [{"fs": right}, {"fs": left}]
+    greet += [{"fs": ring((pos + k) % m)} for k in range(1, m)]
     for device in greet:
         pl.semaphore_signal(barrier, inc=1, device_id=device, device_id_type=MESH)
 
+    def span(w, part):
+        block = shards[w].shape[0]
+        tail = block // 8 // 16 * 16
+        head = block - tail
+        cut = -(-head // 32) * 16
+        if w % 2:
+            cut = head - cut
+        return {"all": (0, block), None: (0, head), 0: (0, cut), 1: (cut, head - cut),
+                2: (head, tail)}[part]
+
     def region(w, p, q, part=None):
-        block = shards[w].shape[0]
-        at = (((sp + p) % n) * m + ring((pos + q + m) % m)) * block
-        if part is None:
-            return bufs[w].at[pl.ds(pl.multiple_of(at, block), block)]
-        half = block // 2
-        return bufs[w].at[pl.ds(pl.multiple_of(at + part * half, half), half)]
+        lo, size = span(w, part)
+        at = (((sp + p) % n) * m + ring((pos + q + m) % m)) * shards[w].shape[0] + lo
+        return bufs[w].at[pl.ds(pl.multiple_of(at, 16), size)]
+
+    def own(w, part=None):
+        lo, size = span(w, part)
+        return shards[w].at[pl.ds(lo, size)]
+
+    has_tail = span(0, 2)[1] > 0 and m > 1
 
     started = []
 
@@ -73,12 +85,12 @@
 
     def first(w, k):
         return pltpu.make_async_remote_copy(
-            src_ref=shards[w], dst_ref=region(w, 0, 0), send_sem=s1.at[w * n + k],
+            src_ref=own(w), dst_ref=region(w, 0, 0), send_sem=s1.at[w * n + k],
             recv_sem=r1.at[w * n + n - k], device_id={"sp": (sp + k) % n}, device_id_type=MESH)
 
     def first_wait(w, p):
         pltpu.make_async_remote_copy(
-            src_ref=shards[w], dst_ref=region(w, p, 0), send_sem=s1.at[w * n + p],
+            src_ref=own(w), dst_ref=region(w, p, 0), send_sem=s1.at[w * n + p],
             recv_sem=r1.at[w * n + p], device_id={"sp": (sp + p) % n},
             device_id_type=MESH).wait_recv()
 
@@ -86,10 +98,7 @@
         q = -d if way == 0 else d
         part = way if (m % 2 == 0 and d + 1 == far) else None
         if p == 0 and d == 0:
-            src = shards[w]
-            if part is not None:
-                half = shards[w].shape[0] // 2
-                src = src.at[pl.ds(part * half, half)]
+            src = own(w, part)
         else:
             src = region(w, p, q, part)
         at = ((w * n + p) * 2 + way) * max(far, 1) + d
@@ -118,26 +127,69 @@
                 launch(second(w, p, way, d))
 
     def last_wait(w, p):
+        tail_wait(w, p)
         if far >= 1:
             for way in (0, 1):
                 second_wait(w, p, way, far)
 
+    def tail_one(w, k):
+        return pltpu.make_async_remote_copy(
+            src_ref=own(w, 2), dst_ref=region(w, 0, 0, 2), send_sem=t1s.at[w * m + k],
+            recv_sem=t1r.at[w * m + m - k], device_id={"fs": ring((pos + k) % m)},
+            device_id_type=MESH)
+
+    def tail_one_wait(w, q):
+        ref = region(w, 0, q, 2)
+        pltpu.make_async_remote_copy(
+            src_ref=ref, dst_ref=ref, send_sem=t1s.at[w * m + q], recv_sem=t1r.at[w * m + q],
+            device_id={"fs": ring((pos + q) % m)}, device_id_type=MESH).wait_recv()
+
+    def tail_two(w, q, k):
+        at = (w * m + q) * n
+        return pltpu.make_async_remote_copy(
+            src_ref=own(w, 2) if q == 0 else region(w, 0, q, 2), dst_ref=region(w, 0, q, 2),
+            send_sem=t2s.at[at + k], recv_sem=t2r.at[at + n - k],
+            device_id={"sp": (sp + k) % n}, device_id_type=MESH)
+
+    def tail_start(w):
+        if has_tail:
+            for k in range(1, m):
+                launch(tail_one(w, k))
+
+    def tail_forward(w):
+        if has_tail:
+            for q in range(m):
+                if q:
+                    tail_one_wait(w, q)
+                for k in order:
+                    launch(tail_two(w, q, k))
+
+    def tail_wait(w, p):
+        if has_tail and p:
+            for q in range(m):
+                ref = region(w, p, q, 2)
+                at = (w * m + q) * n + p
+                pltpu.make_async_remote_copy(
+                    src_ref=ref, dst_ref=ref, send_sem=t2s.at[at], recv_sem=t2r.at[at],
+                    device_id={"sp": (sp + p) % n}, device_id_type=MESH).wait_recv()
+
+    order = sorted(range(1, n), key=lambda p: min(p, n - p))
     local = [
         pltpu.make_async_copy(tokens, raw, loc.at[0]),
         pltpu.make_async_copy(shift_hbm, shift, loc.at[1]),
         pltpu.make_async_copy(rgate, rg, loc.at[2]),
         pltpu.make_async_copy(igate, ig, loc.at[3]),
         pltpu.make_async_copy(pmix, pm, loc.at[4]),
-    ] + [pltpu.make_async_copy(shards[w], region(w, 0, 0), loc.at[5 + w]) for w in range(4)]
+    ] + [pltpu.make_async_copy(shards[w], region(w, 0, 0, "all"), loc.at[5 + w]) for w in range(4)]
     for copy in local:
         copy.start()
 
     pl.semaphore_wait(barrier, len(greet))
-    order = sorted(range(1, n), key=lambda p: min(p, n - p))
     for w in (0, 1):
         second_all(w, 0)
         for k in order:
             launch(first(w, k))
+        tail_start(w)
 
     local[0].wait()
     mine = tp * half_rows
@@ -164,9 +216,12 @@
             second_all(w, p)
         if p == order[0]:
             launch(normed_copy(tp))
+    for w in (0, 1):
+        tail_forward(w)
     for w in (2, 3):
         for k in order:
             launch(first(w, k))
+        tail_start(w)
     for p in [0] + order:
         for w in (0, 1):
             forward(w, p)
@@ -179,6 +234,8 @@
         for w in (2, 3):
             first_wait(w, p)
             second_all(w, p)
+    for w in (2, 3):
+        tail_forward(w)
     for copy in local[1:]:
         copy.wait()
     normed_copy(1 - tp).wait_recv()
@@ -333,16 +390,17 @@
 
         lax.fori_loop(0, rows // ROWS, fix, 0)
 
-    for p in [0] + order:
-        for w in (2, 3):
-            last_wait(w, p)
-
-    out_count = width // COLS
     dims = (((1,), (1,)), ((), ()))
+    out_cols = sendbuf.shape[2]
+    out_count = width // out_cols
+    per_group = m * chain_exit.shape[0] // out_cols
+
+    def out_lanes(j):
+        return pl.ds(pl.multiple_of(j * out_cols, out_cols), out_cols)
 
     def partial(owner, j):
         at = pl.ds(pl.multiple_of(owner * half_rows, ROWS), half_rows)
-        b = lanes(j)
+        b = out_lanes(j)
         x = rec[:, at, :].reshape(seqs * half_rows, chans)
         y = pooled[:, at, :].reshape(seqs * half_rows, chans)
         return lax.dot_general(x, w2[b, :], dims, preferred_element_type=F32) + lax.dot_general(
@@ -359,15 +417,25 @@
         out_copy(j).start()
         return c
 
-    lax.fori_loop(0, out_count, exit_step, 0)
-
     def out_step(j, c):
         out_copy(j).wait_recv()
         total = (acc[j] + recvbuf[j].astype(F32)).astype(BF16)
-        out[:, :, lanes(j)] = total.reshape(seqs, half_rows, COLS)
+        out[:, :, out_lanes(j)] = total.reshape(seqs, half_rows, out_cols)
         return c
 
-    lax.fori_loop(0, out_count, out_step, 0)
+    def group(p, step):
+        j = ((sp + p) % n) * per_group
+        lax.fori_loop(j, j + per_group, step, 0)
+
+    before = None
+    for p in [0] + order:
+        for w in (2, 3):
+            last_wait(w, p)
+        group(p, exit_step)
+        if before is not None:
+            group(before, out_step)
+        before = p
+    group(before, out_step)
 
     def out_end(j, c):
         out_copy(j).wait_send()
@@ -399,7 +467,8 @@
     hbm, vmem = pl.BlockSpec(memory_space=pl.ANY), pl.BlockSpec(memory_space=pltpu.VMEM)
     dma = pltpu.SemaphoreType.DMA
     ab_rows = -(-2 * seqs // 8) * 8
-    out_count = width // COLS
+    out_cols = min(COLS, m * chain_exit.shape[1])
+    out_count = width // out_cols
     scratch = [pltpu.VMEM((width, chans), BF16)] * 4 + [
         pltpu.VMEM((seqs, half_rows, width), BF16),
         pltpu.VMEM((seqs, rows, width), BF16),
@@ -419,10 +488,11 @@
         pltpu.VMEM((ab_rows, chans), F32),
         pltpu.VMEM((n, ab_rows, chans), F32),
         pltpu.VMEM((seqs, chans), F32),
-        pltpu.VMEM((out_count, seqs * half_rows, COLS), F32),
-        pltpu.VMEM((out_count, seqs * half_rows, COLS), BF16),
-        pltpu.VMEM((out_count, seqs * half_rows, COLS), BF16),
+        pltpu.VMEM((out_count, seqs * half_rows, out_cols), F32),
+        pltpu.VMEM((out_count, seqs * half_rows, out_cols), BF16),
+        pltpu.VMEM((out_count, seqs * half_rows, out_cols), BF16),
         dma((4 * n,)), dma((4 * n,)), dma((8 * n * far,)), dma((8 * n * far,)),
+        dma((4 * m,)), dma((4 * m,)), dma((4 * m * n,)), dma((4 * m * n,)),
         dma((9,)), dma((2,)), dma((2,)), dma((2,)), dma((n,)), dma((n,)),
         dma((out_count,)), dma((out_count,)),
     ]

time: 183 us -> 170 us (0.929)
  the two profiles are of different devices: /device:TPU:11 before, /device:TPU:23 now
where the time goes in v2:
time: 170 us
  Pallas kernels  164 us (96%)
  local copies, waits for them, and re-layouts  6.31 us (4%)
    pallas_call x1, Pallas kernels, per_device(): pl.pallas_call(functools.partial(kernel, n, m), name='layer', out_shape=j...  164 us
    unnamed x3, local copies, waits for them, and re-layouts  6.31 us

profile of v2, /device:TPU:23, one launch (start us, length us, event | category | flops | bytes accessed | tf_op | source)
XLA Modules:
  0.0 169.9 jit_solution(17370708330373236284)
XLA Ops:
  0.0 1.8 %copy.15 = bf16[1024,128]{0,1:T(8,128)(2,1)} copy(bf16[1024,128]{1,0:T(8,128)(2,1)} %param.26) | data formatting | bytes 524288 | tf_op args[12]
  1.8 1.8 %copy.16 = bf16[1024,128]{0,1:T(8,128)(2,1)} copy(bf16[1024,128]{1,0:T(8,128)(2,1)} %param.27) | data formatting | bytes 524288 | tf_op args[13]
  3.6 163.6 %layer.1 = bf16[2,192,2048]{2,1,0:T(8,128)(2,1)} custom-call(bf16[2,192,2048]{2,1,0:T(8,128)(2,1)} %tokens.1, f32[1,2048]{1,0:T(1,128)} %bitcast.7, bf16[128,1024]{1,0:T(8,128)(2,1)} %chain_entry.1, bf16[128,1024]{1,0:T(8,128)(2,1)} %pool_entry.1, bf16[4,1024]{1,0:T(4,128)(2,1)} %taps.1, bf16[4,256,256]{2,1,0:T(8,128)(2,1)} %rgate.1, ...), custom_call_target="tpu_custom_call" | custom-call | tf_op jit(solution)/shard_map/layer/pallas_call | solution.py:499
  167.2 2.7 %copy.18 = bf16[2,192,2048]{2,1,0:T(8,128)(2,1)} copy(bf16[2,192,2048]{2,1,0:T(8,128)(2,1)} %layer.1) | data formatting | bytes 3145728
